TPU v7x, 256 devices: a whole 4x4x8 slice. The times are simulated.
256 devices in a mesh: ep: 16 (over y, x), tp: 16 (over z, core).
Axes of the slice: x: 4, y: 4, z: 8, core: 2. Of those that a mesh axis runs over, the one named last changes fastest.
Arguments:
- query_rows: bfloat16 [16384, 2048], P('ep', 'tp'), may hold values from -6 to 6
- key_rows: bfloat16 [16384, 2048], P('ep', 'tp'), may hold values from -6 to 6
- value_rows: bfloat16 [16384, 4096], P('ep', 'tp'), may hold values from -6 to 6
- gate_rows: bfloat16 [16384, 4096], P('ep', 'tp'), may hold values from -6 to 6
- log_decay: float32 [16, 16384], P('tp', 'ep'), may hold values from -1.5 to 0
- out_weight: bfloat16 [4096, 2048], P('tp'), may hold values from -0.09375 to 0.09375
- channel_input: bfloat16 [12288, 2048], P(('ep', 'tp')), may hold values from -6 to 6
- norm_gain: float32 [2048], replicated, may hold values from 0.1 to 1.9
- routes: int32 [12288, 2], P(('ep', 'tp')), may hold values from 0 to 31, all different within a row; in each aligned block of 48 rows (0 to 47, 48 to 95, ...) at most 5 rows name the same one
- route_weight: float32 [12288, 2], P(('ep', 'tp')), may hold values from 0.2 to 1.5
- expert_gate: bfloat16 [32, 2048, 2048], P('ep', None, 'tp'), may hold values from -0.125 to 0.125
- expert_up: bfloat16 [32, 2048, 2048], P('ep', None, 'tp'), may hold values from -0.125 to 0.125
- expert_down: bfloat16 [32, 2048, 2048], P('ep', 'tp'), may hold values from -0.125 to 0.125
- shared_gate: bfloat16 [2048, 2048], P(None, 'tp'), may hold values from -0.125 to 0.125
- shared_up: bfloat16 [2048, 2048], P(None, 'tp'), may hold values from -0.125 to 0.125
- shared_down: bfloat16 [2048, 2048], P('tp'), may hold values from -0.125 to 0.125
Outputs:
- mixer_out: bfloat16 [16384, 2048], P(('ep', 'tp'))
- channel_out: bfloat16 [12288, 2048], P(('ep', 'tp'))
Inputs may be any that keep to these rules, and one draw needn't show every extreme that they name: `routes`: each row names 2 different experts; among the rows of one device no expert is named more than 5 times, a bound that some block reaches.
All inputs are finite; a program needn't handle non-finite values.
Results may differ from a plain program's by a relative error of at most 0.02.
Values may be sent and summed in bfloat16 or wider, within the bound.
No kernel may reach another device: no remote copies, remote signals or barrier semaphores. Data moves between devices by JAX's collectives and lax.ppermute only.
A program may use at most 128 MiB of HBM per device.

v0:
```python
import jax
import jax.numpy as jnp
from jax import lax
from jax.sharding import Mesh
from jax.sharding import PartitionSpec as P

BLOCK = 128
EP = ("ep_0", "ep_1")
EP_TP = ("ep_0", "ep_1", "tp")


epsilon = 1e-06
turn_base = 10000.0


def filled_with(array, identity):
    return jax.tree.map(
        lambda a, e: jnp.broadcast_to(jnp.asarray(e, a.dtype), a.shape), array, identity
    )


def carried_in(array, axes, combine, identity):
    before = start = filled_with(array, identity)
    total = array
    for axis in reversed(axes):
        length, index = (lax.axis_size(axis), lax.axis_index(axis))
        pieces = jax.tree.map(
            lambda part, kind: lax.all_gather(part.astype(kind), axis),
            total,
            (jnp.bfloat16, jnp.bfloat16),
        )
        inside, total = (start, start)
        for k in range(length):
            passed = k < index
            total = combine(
                total, jax.tree.map(lambda part, own: part[k].astype(own.dtype), pieces, array)
            )
            inside = jax.tree.map(lambda new, old: jnp.where(passed, new, old), total, inside)
        before = combine(inside, before)
    return before


def turn_heads(rows, position):
    half_width = rows.shape[-1] // 2
    inverse = turn_base ** (-jnp.arange(half_width, dtype=jnp.float32) / half_width)
    angles = position[:, None] * inverse[None, :]
    cosine = jnp.cos(angles)[:, None, :]
    sine = jnp.sin(angles)[:, None, :]
    widened = rows.astype(jnp.float32)
    first_half = widened[..., :half_width]
    second_half = widened[..., half_width:]
    turned = jnp.concatenate(
        [first_half * cosine - second_half * sine, second_half * cosine + first_half * sine],
        axis=-1,
    )
    return turned.astype(jnp.bfloat16)


def chain_states(earlier, later):
    return (earlier[0] + later[0], jnp.exp(later[0])[:, None, None] * earlier[1] + later[1])


def compute_slots(route_rows, expert_count, capacity):
    flat_routes = route_rows.reshape(-1)
    onehot = (flat_routes[:, None] == jnp.arange(expert_count, dtype=jnp.int32)[None, :]).astype(
        jnp.int32
    )
    earlier = jnp.cumsum(onehot, axis=0) - onehot
    ranking = jnp.sum(earlier * onehot, axis=1)
    return flat_routes * capacity + ranking


def dispatch_matrix(slot_flat, tokens_here, topk_count, slot_count):
    hits = jnp.arange(slot_count, dtype=jnp.int32)[:, None] == slot_flat[None, :]
    return jnp.any(hits.reshape(slot_count, tokens_here, topk_count), axis=2).astype(jnp.bfloat16)


def gated_pair(gate_part, up_part):
    return (jax.nn.silu(gate_part) * up_part).astype(jnp.bfloat16)


def local(
    query_rows,
    key_rows,
    value_rows,
    gate_rows,
    log_decay,
    out_weight,
    channel_input,
    norm_gain,
    routes,
    route_weight,
    expert_gate,
    expert_up,
    expert_down,
    shared_gate,
    shared_up,
    shared_down,
):
    tokens_dev = query_rows.shape[0]
    head_count = log_decay.shape[0]
    key_width = query_rows.shape[1] // head_count
    value_width = value_rows.shape[1] // head_count
    block_count = tokens_dev // BLOCK
    position = (lax.axis_index(EP) * tokens_dev + jnp.arange(tokens_dev, dtype=jnp.int32)).astype(
        jnp.float32
    )
    queries = turn_heads(query_rows.reshape(tokens_dev, head_count, key_width), position)
    queries = queries.reshape(block_count, BLOCK, head_count, key_width)
    keys_turned = turn_heads(key_rows.reshape(tokens_dev, head_count, key_width), position)
    keys_turned = keys_turned.reshape(block_count, BLOCK, head_count, key_width)
    values = value_rows.reshape(block_count, BLOCK, head_count, value_width)
    decay = jnp.transpose(log_decay.reshape(head_count, block_count, BLOCK), (1, 2, 0))
    running = jnp.cumsum(decay, axis=1)
    block_end = running[:, -1, :]
    tail = jnp.exp(block_end[:, None, :] - running)
    value_wide = values.astype(jnp.float32)
    updates = jnp.einsum(
        "njhk,njhe->nhke", keys_turned.astype(jnp.float32) * tail[..., None], value_wide
    )

    def advance(carry, inputs):
        block_decay, update = inputs
        return (jnp.exp(block_decay)[:, None, None] * carry + update, carry)

    start_state = jnp.zeros((head_count, key_width, value_width), jnp.float32)
    final_state, state_before = lax.scan(advance, start_state, (block_end, updates))
    device_total = jnp.sum(block_end, axis=0)
    entry_parts = carried_in(
        (device_total, final_state),
        EP,
        chain_states,
        (jnp.zeros_like(device_total), jnp.zeros_like(final_state)),
    )
    entry_state = entry_parts[1]
    offsets = jnp.cumsum(block_end, axis=0) - block_end
    state_before = state_before + jnp.exp(offsets)[:, :, None, None] * entry_state[None]
    scores = jnp.einsum("nihk,njhk->nhij", queries, keys_turned, preferred_element_type=jnp.float32)
    by_head = jnp.transpose(running, (0, 2, 1))
    spread = by_head[:, :, :, None] - by_head[:, :, None, :]
    lower = jnp.arange(BLOCK)[:, None] >= jnp.arange(BLOCK)[None, :]
    weights = jnp.where(lower, scores * jnp.exp(jnp.where(lower, spread, 0.0)), 0.0).astype(
        jnp.bfloat16
    )
    retained = jnp.einsum("nhij,njhe->nihe", weights, values, preferred_element_type=jnp.float32)
    query_wide = queries.astype(jnp.float32)
    retained = retained + jnp.einsum(
        "nihk,nhke->nihe", query_wide * jnp.exp(running)[..., None], state_before
    )
    retained = retained.reshape(tokens_dev, head_count, value_width)
    scaled = retained * lax.rsqrt(jnp.mean(retained * retained, axis=-1, keepdims=True) + epsilon)
    gate_wide = gate_rows.astype(jnp.float32).reshape(tokens_dev, head_count, value_width)
    gated = (
        (jax.nn.silu(gate_wide) * scaled)
        .astype(jnp.bfloat16)
        .reshape(tokens_dev, head_count * value_width)
    )
    tokens_here = channel_input.shape[0]
    topk_count = routes.shape[1]
    model_width = channel_input.shape[1]
    local_experts = expert_gate.shape[0]
    hidden_part = expert_gate.shape[2]
    ep_count = lax.axis_size(EP)
    tp_count = lax.axis_size("tp")
    experts_all = ep_count * local_experts
    capacity = tokens_here * topk_count // experts_all + max(
        2, tokens_here * topk_count // (3 * experts_all)
    )
    slot_count = experts_all * capacity
    widened = channel_input.astype(jnp.float32)
    normed = (
        widened
        * lax.rsqrt(jnp.mean(widened * widened, axis=-1, keepdims=True) + epsilon)
        * norm_gain
    ).astype(jnp.bfloat16)
    own_slots = compute_slots(routes, experts_all, capacity)
    placing = dispatch_matrix(own_slots, tokens_here, topk_count, slot_count)
    outgoing = jnp.dot(placing, normed, preferred_element_type=jnp.float32).astype(jnp.bfloat16)
    outgoing = outgoing.reshape(experts_all, capacity, model_width)
    arrived = lax.all_to_all(outgoing, EP, split_axis=0, concat_axis=0, tiled=True)
    arrived = arrived.reshape(1, ep_count, local_experts, capacity, model_width)
    routed_piece, own_piece = lax.all_gather((arrived, normed[None]), "tp", axis=0, tiled=True)
    count = routed_piece.shape[0]
    routed_gate = jnp.einsum(
        "cejpd,jdf->cejpf", routed_piece, expert_gate, preferred_element_type=jnp.float32
    )
    routed_up = jnp.einsum(
        "cejpd,jdf->cejpf", routed_piece, expert_up, preferred_element_type=jnp.float32
    )
    routed_hidden = gated_pair(routed_gate, routed_up).reshape(count, slot_count, hidden_part)
    own_gate = jnp.einsum("cnd,df->cnf", own_piece, shared_gate, preferred_element_type=jnp.float32)
    own_up = jnp.einsum("cnd,df->cnf", own_piece, shared_up, preferred_element_type=jnp.float32)
    own_hidden = gated_pair(own_gate, own_up)
    hidden_all = jnp.concatenate([routed_hidden, own_hidden], axis=1)
    mixer_count = tokens_dev // tp_count
    mixer_term = jnp.dot(gated, out_weight, preferred_element_type=jnp.float32)
    mixer_term = mixer_term.reshape(lax.axis_size("tp") * 1, mixer_count, model_width)
    routed_hidden = hidden_all[:, :slot_count].reshape(
        lax.axis_size("tp") * 1, ep_count, local_experts, capacity, hidden_part
    )
    routed_term = jnp.einsum(
        "cejpf,jfd->cejpd", routed_hidden, expert_down, preferred_element_type=jnp.float32
    )
    routed_term = routed_term.reshape(lax.axis_size("tp") * 1, slot_count, model_width)
    shared_term = jnp.einsum(
        "cnf,fd->cnd", hidden_all[:, slot_count:], shared_down, preferred_element_type=jnp.float32
    )
    summed = lax.psum_scatter(
        jnp.concatenate([mixer_term, routed_term, shared_term], axis=1).astype(jnp.bfloat16),
        "tp",
        scatter_dimension=0,
        tiled=True,
    ).astype(jnp.float32)
    mixer_out = summed[0, :mixer_count].astype(jnp.bfloat16)
    routed_back = summed[0, mixer_count : mixer_count + slot_count].astype(jnp.bfloat16)
    routed_back = routed_back.reshape(experts_all, capacity, model_width)
    returned = lax.all_to_all(routed_back, EP, split_axis=0, concat_axis=0, tiled=True).reshape(
        slot_count, model_width
    )
    picked = jnp.take(returned, own_slots, axis=0).reshape(tokens_here, topk_count, model_width)
    shared_result = summed[0, mixer_count + slot_count :]
    channel = shared_result + jnp.sum(route_weight[:, :, None] * picked.astype(jnp.float32), axis=1)
    return (mixer_out, channel.astype(jnp.bfloat16))


def solution(mesh):
    split = Mesh(mesh.devices.reshape(4, 4, mesh.shape["tp"]), ("ep_0", "ep_1", "tp"))
    return jax.shard_map(
        local,
        mesh=split,
        in_specs=(
            P(EP, "tp"),
            P(EP, "tp"),
            P(EP, "tp"),
            P(EP, "tp"),
            P("tp", EP),
            P("tp", None),
            P(EP_TP, None),
            P(),
            P(EP_TP, None),
            P(EP_TP, None),
            P(EP, None, "tp"),
            P(EP, None, "tp"),
            P(EP, "tp", None),
            P(None, "tp"),
            P(None, "tp"),
            P("tp", None),
        ),
        out_specs=(P(EP_TP, None), P(EP_TP, None)),
        check_vma=False,
    )
```

profile of v0, /device:TPU:33, one launch (start us, length us, event | category | flops | bytes accessed | tf_op | source)
XLA Modules:
  0.0 378.1 jit_solution(7713296749920263441)
XLA Ops:
  8.4 1.7 fusion.57
  14.1 22.7 %all_to_all.10 = bf16[32,5,2048]{2,1,0:T(8,128)(2,1)S(1)} all-to-all(bf16[32,5,2048]{2,1,0:T(8,128)(2,1)S(1)} %reshape.534), channel_id=1, replica_groups=mesh['ep_0'=4,'ep_1'=4,'tp'=16] {'ep_0','ep_1'}, dimensions={0} | all-to-all | bytes 1310720 | tf_op jit(solution)/shard_map/all_to_all | solution.py:180
  39.1 23.2 %fusion.93 = f32[8,128,1]{2,0,1:T(8,128)S(1)} fusion(f32[8,128,1]{2,0,1:T(8,128)S(1)} %copy.81), kind=kOutput, calls=%fused_computation.151 | output fusion | flops 130048 | bytes 8192 | tf_op jit(solution)/shard_map/jit(cumsum)/reduce_window_sum | solution.py:114
  64.3 6.5 %all-reduce = bf16[4]{0:T(256)(128)(2,1)S(1)} all-reduce(bf16[4]{0:T(256)(128)(2,1)S(1)} %dynamic-update-slice), channel_id=1, replica_groups=mesh['ep_0'=4,'ep_1'=4,'tp'=16] {'ep_1'}, use_global_device_ids=true, to_apply=%add | all-reduce | flops 4 | bytes 16
  73.3 6.9 %all-reduce.1 = bf16[4]{0:T(256)(128)(2,1)S(1)} all-reduce(bf16[4]{0:T(256)(128)(2,1)S(1)} %dynamic-update-slice.1), channel_id=2, replica_groups=mesh['ep_0'=4,'ep_1'=4,'tp'=16] {'ep_0'}, use_global_device_ids=true, to_apply=%add.1 | all-reduce | flops 4 | bytes 16
  80.7 2.5 fusion.34
  83.3 1.7 convolution_bitcast_fusion.2
  84.9 15.8 %while.13 = (s32[]{:T(128)}, f32[1,128,256]{2,1,0:T(8,128)S(1)}, f32[8,1,128,256]{3,2,1,0:T(8,128)}, f32[8,1]{0,1:T(1,128)S(1)}, f32[8,1,128,256]{3,2,1,0:T(8,128)S(1)}, /*index=5*/s32[]{:T(128)}, s32[]{:T(128)}) while((s32[]{:T(128)}, f32[1,128,256]{2,1,0:T(8,128)S(1)}, f32[8,1,128,256]{3,2,1,0:T(8,128)}, f32[8,1]{0,1:T(1,128)S(1)}, ...), condition=%wide.region_2.3_spmd.clone, body=%wide.region_1.2_spmd.clone.sunk | while | flops 131075 | bytes 655980 | solution.py:127
  110.5 9.4 %all-gather.1 = bf16[4,128,256]{2,1,0:T(8,128)(2,1)S(1)} all-gather(bf16[1,128,256]{2,1,0:T(8,128)(2,1)S(1)} %convert_element_type.229), channel_id=3, replica_groups=mesh['ep_0'=4,'ep_1'=4,'tp'=16] {'ep_1'}, dimensions={0}, use_global_device_ids=true | all-gather | bytes 327680 | tf_op jit(solution)/shard_map/all_gather | solution.py:28
  119.9 9.8 %all_gather.34 = bf16[4,1,128,256]{3,2,1,0:T(8,128)(2,1)S(1)} all-gather(bf16[1,1,128,256]{3,2,1,0:T(8,128)(2,1)S(1)} %fusion.73), channel_id=1, replica_groups=mesh['ep_0'=4,'ep_1'=4,'tp'=16] {'ep_0'}, dimensions={0}, use_global_device_ids=true | all-gather | bytes 327680 | tf_op jit(solution)/shard_map/all_gather | solution.py:28
  131.6 1.8 fusion.19
  135.1 4.3 %copy.90 = bf16[16,64,2048]{2,0,1:T(8,128)(2,1)} copy(bf16[16,64,2048]{2,1,0:T(8,128)(2,1)S(1)} %convolution_convert_fusion) | data formatting | bytes 8388608 | tf_op jit(solution)/shard_map/convert.8
  139.4 2.9 fusion.44
  142.4 6.9 %convolution_convert_fusion.1 = bf16[16,48,2048]{2,1,0:T(8,128)(2,1)} fusion(bf16[16,48,2048]{2,1,0:T(8,128)(2,1)} %bitcast.164, bf16[128,2048]{1,0:T(8,128)(2,1)S(1)} %copy-done.6, bf16[2048,128]{1,0:T(8,128)(2,1)S(1)} %copy-done.7, f32[16,48,128]{2,1,0:T(8,128)S(1)} %fusion.44), kind=kOutput, calls=%fused_computation.7 | convolution fusion | flops 807469056 | bytes 7733248 | tf_op jit(solution)/shard_map/cnf,fd->cnd/dot_general | solution.py:205
  149.2 5.4 %copy.91 = bf16[16,48,2048]{2,0,1:T(8,128)(2,1)} copy(bf16[16,48,2048]{2,1,0:T(8,128)(2,1)} %convolution_convert_fusion.1) | data formatting | bytes 6291456 | tf_op jit(solution)/shard_map/convert.10
  154.6 6.0 %convolution_bitcast_fusion.1 = f32[16,16,2,5,128]{4,1,3,0,2:T(8,128)S(1)} fusion(bf16[16,16,2,5,2048]{4,1,3,0,2:T(8,128)(2,1)} %all-gather.6.cloned.1.call-done, bf16[2,2048,128]{2,1,0:T(8,128)(2,1)} %param.28), kind=kOutput, calls=%fused_computation.10 | convolution fusion | flops 1342177280 | bytes 12845056 | tf_op jit(solution)/shard_map/cejpd,jdf->cejpf/dot_general | solution.py:184
  160.6 15.5 %convert_bitcast_fusion = bf16[16,16,2,5,2048]{4,1,3,0,2:T(8,128)(2,1)} fusion(bf16[16,16,2,5,2048]{4,1,3,0,2:T(8,128)(2,1)} %all-gather.6.cloned.1.call-done, f32[16,16,2,5,128]{4,1,3,0,2:T(8,128)S(1)} %convolution_bitcast_fusion.1, bf16[2,128,2048]{2,1,0:T(8,128)(2,1)S(1)} %copy-done, bf16[2,2048,128]{2,1,0:T(8,128)(2,1)S(1)} %copy-done.2), kind=kOutput, calls=%fused_computation.5 | convolution fusion | flops 2691563520 | bytes 24379392 | tf_op jit(solution)/shard_map/cejpf,jfd->cejpd/dot_general | solution.py:201
  176.1 13.8 %copy.89 = bf16[16,16,2,5,2048]{4,0,3,2,1:T(8,128)(2,1)} copy(bf16[16,16,2,5,2048]{4,1,3,0,2:T(8,128)(2,1)} %convert_bitcast_fusion) | data formatting | bytes 20971520 | tf_op jit(solution)/shard_map/cejpf,jfd->cejpd/transpose | solution.py:201
  189.9 8.5 %pad_maximum_fusion = bf16[16,272,2048]{2,0,1:T(8,128)(2,1)S(1)} fusion(bf16[16,48,2048]{2,0,1:T(8,128)(2,1)} %copy.91, bf16[16,160,2048]{2,0,1:T(8,128)(2,1)} %bitcast.162, bf16[16,64,2048]{2,0,1:T(8,128)(2,1)} %copy.90), kind=kLoop, calls=%fused_computation.4 | loop fusion | flops 17825792 | bytes 35651584 | tf_op jit(solution)/shard_map/concatenate | solution.py:209
  198.4 24.4 %copy.92 = bf16[16,272,2048]{2,1,0:T(8,128)(2,1)} copy(bf16[16,272,2048]{2,0,1:T(8,128)(2,1)S(1)} %pad_maximum_fusion) | data formatting | bytes 35651584 | tf_op jit(solution)/shard_map/concatenate | solution.py:209
  223.7 113.9 %reduce-scatter.2.cloned.1.call-done = bf16[1,272,2048]{2,1,0:T(8,128)(2,1)} async-done(((bf16[16,272,2048]{2,1,0:T(8,128)(2,1)}), bf16[1,272,2048]{2,1,0:T(8,128)(2,1)}) %reduce-scatter.2.cloned.1.call-update) | async-done | bytes 1114128 | tf_op jit(solution)/shard_map/reduce_scatter | solution.py:208
  339.9 6.5 %all-to-all-start.1 = ((bf16[32,5,2048]{2,1,0:T(8,128)(2,1)}), bf16[32,5,2048]{2,1,0:T(8,128)(2,1)S(1)}, u32[]{:S(2)}, u32[]{:S(2)}) async-start(bf16[32,5,2048]{2,1,0:T(8,128)(2,1)} %convert_element_type.248), calls=%async_computation.2 | async-start | bytes 2097152 | tf_op jit(solution)/shard_map/all_to_all | solution.py:217
  348.4 18.1 %all-to-all-done.1 = bf16[32,5,2048]{2,1,0:T(8,128)(2,1)S(1)} async-done(((bf16[32,5,2048]{2,1,0:T(8,128)(2,1)}), bf16[32,5,2048]{2,1,0:T(8,128)(2,1)S(1)}, u32[]{:S(2)}, u32[]{:S(2)}) %all-to-all-start.1) | async-done | bytes 655392 | tf_op jit(solution)/shard_map/all_to_all | solution.py:217
  367.8 2.0 multiply_reduce_fusion
  (118 shorter events, 41.1 us)
Async XLA Ops:
  7.2 153.4 %copy-start = (bf16[2,128,2048]{2,1,0:T(8,128)(2,1)S(1)}, bf16[2,128,2048]{2,1,0:T(8,128)(2,1)}, u32[]{:S(2)}) copy-start(bf16[2,128,2048]{2,1,0:T(8,128)(2,1)} %param.30) | copy-start | bytes 3145732
  7.2 132.2 %all-gather.8.cloned.1.call-start = ((), (), s32[]{:S(2)}) async-start(), calls=%async_computation.5 | async-start | bytes 3342336 | tf_op jit(solution)/shard_map/all_gather | solution.py:182
  10.1 144.5 %all-gather.6.cloned.1.call-start = ((), (), s32[]{:S(2)}) async-start(), calls=%async_computation.3 | async-start | bytes 11141120 | tf_op jit(solution)/shard_map/all_gather | solution.py:182
  13.8 24.4 %copy-start.11 = (f32[1,1024]{1,0:T(1,128)S(1)}, f32[1,1024]{1,0:T(1,128)}, u32[]{:S(2)}) copy-start(f32[1,1024]{1,0:T(1,128)} %param.22) | copy-start | bytes 12292
  13.8 24.7 %copy-start.14 = (u32[256]{0:T(256)S(1)}, u32[256]{0:T(256)}, u32[]{:S(2)}) copy-start(u32[256]{0:T(256)} %constant.103) | copy-start | bytes 3076
  14.1 56.7 %copy-start.13 = (u32[256]{0:T(256)S(1)}, u32[256]{0:T(256)}, u32[]{:S(2)}) copy-start(u32[256]{0:T(256)} %constant.108) | copy-start | bytes 3076
  14.1 66.5 %copy-start.8 = (bf16[1024,128]{1,0:T(8,128)(2,1)S(1)}, bf16[1024,128]{1,0:T(8,128)(2,1)}, u32[]{:S(2)}) copy-start(bf16[1024,128]{1,0:T(8,128)(2,1)} %param.19) | copy-start | bytes 786436
  14.1 66.5 %copy-start.9 = (bf16[1024,128]{1,0:T(8,128)(2,1)S(1)}, bf16[1024,128]{1,0:T(8,128)(2,1)}, u32[]{:S(2)}) copy-start(bf16[1024,128]{1,0:T(8,128)(2,1)} %param.18) | copy-start | bytes 786436
  38.1 299.4 %reduce-scatter.2.cloned.1.call-start = ((), (), s32[]{:S(2)}) async-start(), calls=%async_computation.4 | async-start | bytes 18939904 | tf_op jit(solution)/shard_map/reduce_scatter | solution.py:208
  131.6 1.9 copy-start.4
  131.6 2.3 copy-start.3
  135.1 4.3 %copy-start.5 = (bf16[2048,128]{1,0:T(8,128)(2,1)S(1)}, bf16[2048,128]{1,0:T(8,128)(2,1)}, u32[]{:S(2)}) copy-start(bf16[2048,128]{1,0:T(8,128)(2,1)} %param.31) | copy-start | bytes 1572868
  139.4 3.0 copy-start.6
  139.4 3.0 copy-start.7
  154.6 6.0 %copy-start.2 = (bf16[2,2048,128]{2,1,0:T(8,128)(2,1)S(1)}, bf16[2,2048,128]{2,1,0:T(8,128)(2,1)}, u32[]{:S(2)}) copy-start(bf16[2,2048,128]{2,1,0:T(8,128)(2,1)} %param.29) | copy-start | bytes 3145732
  222.8 0.7 copy-start.10
  223.4 123.2 %copy-start.12 = (f32[48,2]{0,1:T(2,128)S(1)}, f32[48,2]{0,1:T(2,128)}, u32[]{:S(2)}) copy-start(f32[48,2]{0,1:T(2,128)} %param.27) | copy-start | bytes 1156
  339.9 26.5 %all-to-all-start.1 = ((bf16[32,5,2048]{2,1,0:T(8,128)(2,1)}), bf16[32,5,2048]{2,1,0:T(8,128)(2,1)S(1)}, u32[]{:S(2)}, u32[]{:S(2)}) async-start(bf16[32,5,2048]{2,1,0:T(8,128)(2,1)} %convert_element_type.248), calls=%async_computation.2 | async-start | bytes 2097152 | tf_op jit(solution)/shard_map/all_to_all | solution.py:217
  366.4 5.1 %copy-start.1 = (bf16[2,128,2048]{2,1,0:T(8,128)(2,1)S(1)}, bf16[2,128,2048]{2,1,0:T(8,128)(2,1)}, u32[]{:S(2)}) copy-start(bf16[2,128,2048]{2,1,0:T(8,128)(2,1)} %param.30) | copy-start | bytes 3145732
Sparse Core Ops, SparseCore 0:
  10.4 43.3 all-gather.7
  55.6 62.6 all-gather.5
  222.9 114.5 reduce-scatter.1
where the time goes:
time: 379 us; the launch traced here: 378 us
  waiting for transfers between devices  132 us (35%)
  local copies, waits for them, and re-layouts  67.1 us (18%)
  other arithmetic  55.6 us (15%)
  blocking collectives  55.3 us (15%)
  matrix products  38.9 us (10%)
  between operations  22.3 us (6%)
  starting transfers between devices  6.65 us (2%)
    reduce_scatter x1, waiting for transfers between devices, local(): lax.psum_scatter(jnp.concatenate([mixer_term, routed_term, shared_term],...  114 us
    concatenate x1, local copies, waits for them, and re-layouts, local(): jnp.concatenate([mixer_term, routed_term, shared_term], axis=1)  24.4 us
    another operation x1, other arithmetic, local(): running = jnp.cumsum(decay, axis=1)  23.2 us
    all_to_all x1, blocking collectives, local(): lax.all_to_all(outgoing, EP, split_axis=0, concat_axis=0, tiled=True)  22.7 us
    all_gather x2, blocking collectives, carried_in(): lax.all_gather(part.astype(kind), axis)  19.2 us
    all_to_all x1, waiting for transfers between devices, local(): lax.all_to_all(routed_back, EP, split_axis=0, concat_axis=0, tiled=True)  18.1 us
    dot_general x1, matrix products, local(): jnp.einsum('cejpf,jfd->cejpd', routed_hidden, expert_down, preferred_elem...  15.5 us
    transpose x1, local copies, waits for them, and re-layouts, local(): jnp.einsum('cejpf,jfd->cejpd', routed_hidden, expert_down, preferred_elem...  13.8 us
  transfers between devices with their start and end apart: 4, of which 2 were waited for; matrix products, arithmetic and copies ran while one was open for 22% of the time, Pallas kernels for 0%

commit v1 on v0

v1 whole, which is shorter than its diff:
```python
import jax
import jax.numpy as jnp
from jax import lax
from jax.experimental import pallas as pl
from jax.experimental.pallas import tpu as pltpu
from jax.sharding import Mesh
from jax.sharding import PartitionSpec as P

BLOCK = 128
EP = ("ep_0", "ep_1")
EP_TP = ("ep_0", "ep_1", "tp")
LANES = 128
SLOTS = 8

epsilon = 1e-06
turn_base = 10000.0
bf16 = jnp.bfloat16
f32 = jnp.float32


def carried_in(log_total, state, axes):
    before_log, before = jnp.zeros_like(log_total), jnp.zeros_like(state)
    for axis in reversed(axes):
        length, index = lax.axis_size(axis), lax.axis_index(axis)
        high = log_total.astype(bf16)
        low = (log_total - high.astype(f32)).astype(bf16)
        width = state.shape[1]
        marks = jnp.arange(16)[:, None]
        extra = jnp.where(marks == 0, high, jnp.where(marks == 1, low, jnp.zeros((), bf16)))
        packed = jnp.concatenate([state.astype(bf16), jnp.broadcast_to(extra, (16, width))], axis=0)
        pieces = lax.all_gather(packed, axis)
        rows = state.shape[0]
        inside_log, inside = jnp.zeros_like(log_total), jnp.zeros_like(state)
        total_log, total = inside_log, inside
        for k in range(length):
            passed = k < index
            piece_log = pieces[k, rows, 0].astype(f32) + pieces[k, rows + 1, 0].astype(f32)
            total = jnp.exp(piece_log) * total + pieces[k, :rows].astype(f32)
            total_log = total_log + piece_log
            inside = jnp.where(passed, total, inside)
            inside_log = jnp.where(passed, total_log, inside_log)
        before = jnp.exp(before_log) * inside + before
        before_log = before_log + inside_log
        log_total, state = total_log, total
    return before


def turn_tables(position, half_width):
    inverse = turn_base ** (-jnp.arange(half_width, dtype=f32) / half_width)
    angles = position[:, None] * inverse[None, :]
    return jnp.cos(angles), jnp.sin(angles)


def turn_head(rows, cosine, sine):
    half_width = rows.shape[-1] // 2
    widened = rows.astype(f32)
    first_half, second_half = widened[:, :half_width], widened[:, half_width:]
    turned = jnp.concatenate(
        [first_half * cosine - second_half * sine, second_half * cosine + first_half * sine],
        axis=-1,
    )
    return turned.astype(bf16)


def silu(v):
    return v / (1.0 + jnp.exp(-v))


def mixer_kernel(gated_ref, weight_ref, out_ref):
    groups, rows, width = gated_ref.shape
    left = gated_ref[...].reshape(groups * rows, width)
    product = jnp.dot(left, weight_ref[...], preferred_element_type=f32)
    out_ref[...] = product.astype(bf16).reshape(out_ref.shape)


def expert_kernel(x_ref, first_ref, down_ref, held_ref, out_ref):
    del held_ref
    groups, rows, width = x_ref.shape
    model_width = out_ref.shape[-1]
    x = x_ref[...].reshape(groups * rows, width)
    hidden = jnp.dot(x[:, :model_width], first_ref[0], preferred_element_type=f32)
    part = hidden.shape[1] // 4
    extra = x[:, model_width:].astype(f32)
    weight = extra[:, 0:1] + extra[:, 1:2]
    own = extra[:, 2:3]
    routed = silu(hidden[:, :part]) * hidden[:, part : 2 * part] * weight
    shared = silu(hidden[:, 2 * part : 3 * part]) * hidden[:, 3 * part :] * own
    both = jnp.concatenate([routed, shared], axis=1).astype(bf16)
    product = jnp.dot(both, down_ref[0], preferred_element_type=f32)
    out_ref[...] = product.astype(bf16).reshape(out_ref.shape)


def retention(query_rows, key_rows, value_rows, gate_rows, log_decay):
    tokens = query_rows.shape[0]
    count = tokens // BLOCK
    start = lax.axis_index(EP) * tokens
    position = (start + jnp.arange(tokens, dtype=jnp.int32)).astype(f32)
    cosine, sine = turn_tables(position, query_rows.shape[1] // 2)
    queries = turn_head(query_rows, cosine, sine).reshape(count, BLOCK, -1)
    keys_turned = turn_head(key_rows, cosine, sine).reshape(count, BLOCK, -1)
    values = value_rows.reshape(count, BLOCK, -1)
    decay = log_decay.reshape(count, BLOCK)
    lower = jnp.arange(BLOCK)[:, None] >= jnp.arange(BLOCK)[None, :]
    running = jnp.dot(decay, lower.T.astype(f32), precision=lax.Precision.HIGHEST)
    block_end = running[:, -1]
    tail = jnp.exp(block_end[:, None] - running)
    updates = jnp.einsum(
        "njk,nje->nke",
        (keys_turned.astype(f32) * tail[..., None]).astype(bf16),
        values,
        preferred_element_type=f32,
    )
    state = jnp.zeros(updates.shape[1:], f32)
    before = []
    for n in range(count):
        before.append(state)
        state = jnp.exp(block_end[n]) * state + updates[n]
    entry = carried_in(jnp.sum(block_end), state, EP)
    offsets = jnp.cumsum(block_end) - block_end
    state_before = jnp.stack(before) + jnp.exp(offsets)[:, None, None] * entry[None]
    scores = jnp.einsum("nik,njk->nij", queries, keys_turned, preferred_element_type=f32)
    spread = running[:, :, None] - running[:, None, :]
    weights = jnp.where(lower, scores * jnp.exp(jnp.where(lower, spread, 0.0)), 0.0).astype(bf16)
    retained = jnp.einsum("nij,nje->nie", weights, values, preferred_element_type=f32)
    retained = retained + jnp.einsum(
        "nik,nke->nie",
        (queries.astype(f32) * jnp.exp(running)[..., None]).astype(bf16),
        state_before.astype(bf16),
        preferred_element_type=f32,
    )
    retained = retained.reshape(tokens, -1)
    scaled = retained * lax.rsqrt(jnp.mean(retained * retained, axis=-1, keepdims=True) + epsilon)
    return (jax.nn.silu(gate_rows.astype(f32)) * scaled).astype(bf16)


def local(
    query_rows,
    key_rows,
    value_rows,
    gate_rows,
    log_decay,
    out_weight,
    channel_input,
    norm_gain,
    routes,
    route_weight,
    expert_gate,
    expert_up,
    expert_down,
    shared_gate,
    shared_up,
    shared_down,
):
    tokens_dev = query_rows.shape[0]
    tokens_here, topk = routes.shape
    model_width = channel_input.shape[1]
    local_experts, _, hidden_part = expert_gate.shape
    ep_count = lax.axis_size(EP)
    tp_count = lax.axis_size("tp")
    experts_all = ep_count * local_experts
    picks = tokens_here * topk
    capacity = picks // experts_all + max(2, picks // (3 * experts_all))
    slot_count = experts_all * SLOTS

    widened = channel_input.astype(f32)
    normed = (
        widened * lax.rsqrt(jnp.mean(widened * widened, axis=-1, keepdims=True) + epsilon) * norm_gain
    ).astype(bf16)
    flat = routes.reshape(-1)
    order = jnp.arange(picks, dtype=jnp.int32)
    same = (flat[:, None] == flat[None, :]) & (order[None, :] < order[:, None])
    slots = flat * SLOTS + jnp.sum(same.astype(jnp.int32), axis=1)
    placing = (jnp.arange(slot_count, dtype=jnp.int32)[:, None] == slots[None, :]).astype(bf16)
    placing_rows = placing.reshape(slot_count, tokens_here, topk).sum(axis=2)
    flat_weight = route_weight.reshape(-1)
    high = flat_weight.astype(bf16)
    low = (flat_weight - high.astype(f32)).astype(bf16)
    mark = (order % topk == 0).astype(bf16)
    lane = jnp.arange(LANES)[None, :]
    extra = jnp.where(
        lane == 0,
        high[:, None],
        jnp.where(lane == 1, low[:, None], jnp.where(lane == 2, mark[:, None], jnp.zeros((), bf16))),
    )
    outgoing = jnp.concatenate(
        [
            jnp.dot(placing_rows, normed, preferred_element_type=f32).astype(bf16),
            jnp.dot(placing, extra, preferred_element_type=f32).astype(bf16),
        ],
        axis=1,
    )
    width = model_width + LANES
    outgoing = outgoing.reshape(ep_count, local_experts * SLOTS, width)
    arrived = lax.all_to_all(outgoing, EP, split_axis=0, concat_axis=0, tiled=True)
    arrived = arrived.reshape(ep_count, local_experts, SLOTS, width)[:, :, :capacity]
    arrived = jnp.transpose(arrived, (1, 2, 0, 3)).reshape(1, -1, width)
    gathered = lax.all_gather(arrived, "tp", axis=0, tiled=True)
    routed_rows = gathered.shape[1]

    gated = retention(query_rows, key_rows, value_rows, gate_rows, log_decay)
    mixer_rows = tokens_dev // tp_count
    total_rows = routed_rows + mixer_rows
    step = 32
    buffer = pl.pallas_call(
        mixer_kernel,
        grid=(mixer_rows // step,),
        in_specs=[
            pl.BlockSpec((tp_count, step, gated.shape[1]), lambda i: (0, i, 0)),
            pl.BlockSpec(out_weight.shape, lambda i: (0, 0)),
        ],
        out_specs=pl.BlockSpec(
            (tp_count, step, model_width), lambda i: (0, routed_rows // step + i, 0)
        ),
        out_shape=jax.ShapeDtypeStruct((tp_count, total_rows, model_width), bf16),
    )(gated.reshape(tp_count, mixer_rows, -1), out_weight)

    spread = (local_experts,) + shared_gate.shape
    first = jnp.concatenate(
        [
            expert_gate,
            expert_up,
            jnp.broadcast_to(shared_gate, spread),
            jnp.broadcast_to(shared_up, spread),
        ],
        axis=2,
    )
    down = jnp.concatenate(
        [expert_down, jnp.broadcast_to(shared_down, (local_experts,) + shared_down.shape)], axis=1
    )
    each = routed_rows // local_experts
    groups = 4
    buffer = pl.pallas_call(
        expert_kernel,
        grid=(local_experts, tp_count // groups),
        in_specs=[
            pl.BlockSpec((groups, each, width), lambda e, t: (t, e, 0)),
            pl.BlockSpec((1,) + first.shape[1:], lambda e, t: (e, 0, 0)),
            pl.BlockSpec((1,) + down.shape[1:], lambda e, t: (e, 0, 0)),
            pl.BlockSpec(memory_space=pl.ANY),
        ],
        out_specs=pl.BlockSpec((groups, each, model_width), lambda e, t: (t, e, 0)),
        out_shape=jax.ShapeDtypeStruct(buffer.shape, bf16),
        input_output_aliases={3: 0},
        compiler_params=pltpu.CompilerParams(vmem_limit_bytes=50 * 2**20),
    )(gathered, first, down, buffer)

    summed = lax.psum_scatter(buffer, "tp", scatter_dimension=0, tiled=True)[0]
    mixer_out = summed[routed_rows:]
    back = summed[:routed_rows].reshape(local_experts, capacity, ep_count, model_width)
    back = jnp.transpose(back, (2, 0, 1, 3))
    back = jnp.pad(back, ((0, 0), (0, 0), (0, SLOTS - capacity), (0, 0)))
    back = back.reshape(ep_count, local_experts * SLOTS, model_width)
    returned = lax.all_to_all(back, EP, split_axis=0, concat_axis=0, tiled=True)
    returned = returned.reshape(slot_count, model_width)
    channel = jnp.dot(placing_rows.T, returned, preferred_element_type=f32)
    return (mixer_out, channel.astype(bf16))


def solution(mesh):
    split = Mesh(mesh.devices.reshape(4, 4, mesh.shape["tp"]), ("ep_0", "ep_1", "tp"))
    return jax.shard_map(
        local,
        mesh=split,
        in_specs=(
            P(EP, "tp"),
            P(EP, "tp"),
            P(EP, "tp"),
            P(EP, "tp"),
            P("tp", EP),
            P("tp", None),
            P(EP_TP, None),
            P(),
            P(EP_TP, None),
            P(EP_TP, None),
            P(EP, None, "tp"),
            P(EP, None, "tp"),
            P(EP, "tp", None),
            P(None, "tp"),
            P(None, "tp"),
            P("tp", None),
        ),
        out_specs=(P(EP_TP, None), P(EP_TP, None)),
        check_vma=False,
    )
```

time: 379 us -> 250 us (0.66)
  local copies, waits for them, and re-layouts: 67.1 us -> 13.5 us
  other arithmetic: 55.6 us -> 15.9 us
  matrix products: 38.9 us -> 5.67 us
  Pallas kernels: 0 us -> 20.3 us
  waiting for transfers between devices: 132 us -> 112 us
  blocking collectives: 55.3 us -> 43.5 us
  between operations: 22.3 us -> 31.8 us
    dot_general x9 -> x7, matrix products: 38.9 us -> 5.67 us  [the longest x1 1.75 us: retention(): jnp.einsum('nik,nke->nie', (queries.astype(f32) * jnp.exp(running)[..., N...]
    concatenate x1 -> x2, local copies, waits for them, and re-layouts: 24.4 us -> 0.02 us  [carried_in(): jnp.concatenate([state.astype(bf16), jnp.broadcast_to(extra, (16, width))...]
    reduce_scatter x1, waiting for transfers between devices: 114 us -> 91 us  [local(): summed = lax.psum_scatter(buffer, 'tp', scatter_dimension=0, tiled=True)[0]]
    another operation x4, other arithmetic: 26.1 us -> 3.34 us  [the longest x1 23.2 us: local(): running = jnp.cumsum(decay, axis=1)]
    pallas_call x0 -> x2, Pallas kernels: none -> 20.3 us  [the longest x1 16.1 us: local(): pl.pallas_call(expert_kernel, grid=(local_experts, tp_count // groups), i...]
    transpose x1 -> x0, local copies, waits for them, and re-layouts: 13.8 us -> none  [local(): jnp.einsum('cejpf,jfd->cejpd', routed_hidden, expert_down, preferred_elem...]
    unnamed x2 -> x0, blocking collectives: 13.4 us -> none
    another operation x4 -> x0, local copies, waits for them, and re-layouts: 10.1 us -> none
  transfers between devices with their start and end apart: 4 -> 3, of which waited for: 2 -> 3; matrix products, arithmetic and copies ran while one was open for 22% -> 9% of each run, Pallas kernels for 0% -> 2%
where the time goes in v1:
time: 250 us
  waiting for transfers between devices  112 us (45%)
  blocking collectives  43.5 us (17%)
  between operations  31.8 us (13%)
  Pallas kernels  20.3 us (8%)
  other arithmetic  15.9 us (6%)
  local copies, waits for them, and re-layouts  13.5 us (5%)
  starting transfers between devices  6.59 us (3%)
  matrix products  5.67 us (2%)
    reduce_scatter x1, waiting for transfers between devices, local(): summed = lax.psum_scatter(buffer, 'tp', scatter_dimension=0, tiled=True)[0]  91 us
    all_to_all x1, blocking collectives, local(): lax.all_to_all(outgoing, EP, split_axis=0, concat_axis=0, tiled=True)  23.5 us
    all_gather x2, blocking collectives, carried_in(): pieces = lax.all_gather(packed, axis)  20 us
    all_to_all x1, waiting for transfers between devices, local(): returned = lax.all_to_all(back, EP, split_axis=0, concat_axis=0, tiled=True)  18.3 us
    pallas_call x1, Pallas kernels, local(): pl.pallas_call(expert_kernel, grid=(local_experts, tp_count // groups), i...  16.1 us
    unnamed x28, local copies, waits for them, and re-layouts  6.78 us
    all_to_all x1, starting transfers between devices, local(): returned = lax.all_to_all(back, EP, split_axis=0, concat_axis=0, tiled=True)  6.5 us
  transfers between devices with their start and end apart: 3, of which 3 were waited for; matrix products, arithmetic and copies ran while one was open for 9% of the time, Pallas kernels for 2%

profile of v1, /device:TPU:33, one launch (start us, length us, event | category | flops | bytes accessed | tf_op | source)
XLA Modules:
  0.0 249.5 jit_solution(9197828414892601414)
XLA Ops:
  7.3 0.8 copy.53
  8.5 1.1 fusion.29
  9.6 0.8 copy.55
  11.4 1.5 convolution_convert_fusion
  13.2 23.5 %all_to_all.10 = bf16[16,16,2176]{2,1,0:T(8,128)(2,1)S(1)} all-to-all(bf16[16,16,2176]{2,1,0:T(8,128)(2,1)S(1)} %bitcast.64), channel_id=1, replica_groups=mesh['ep_0'=4,'ep_1'=4,'tp'=16] {'ep_0','ep_1'}, dimensions={0} | all-to-all | bytes 2228224 | tf_op jit(solution)/shard_map/all_to_all | solution.py:194
  36.7 1.0 copy.62
  46.9 2.5 %fusion.17 = (bf16[1024,64]{1,0:T(8,128)(2,1)S(1)}, bf16[1024,64]{1,0:T(8,128)(2,1)S(1)}, bf16[1024,64]{1,0:T(8,128)(2,1)S(1)}, bf16[1024,64]{1,0:T(8,128)(2,1)S(1)}) fusion(f32[1024,128]{1,0:T(8,128)S(1)} %convert_element_type.242, f32[64]{0:T(128)S(1)} %multiply_power_fusion, f32[1024]{0:T(1024)S(1)} %add_convert_fusion.2, ...), kind=kLoop, calls=%fused_computation.34 | loop fusion | flops 1114112 | bytes 1577216 | tf_op jit(solution)/shard_map/convert.10
  50.8 10.0 %all-gather = bf16[576,256]{1,0:T(8,128)(2,1)S(1)} all-gather(bf16[144,256]{1,0:T(8,128)(2,1)S(1)} %pad_maximum_fusion.5), channel_id=2, replica_groups=mesh['ep_0'=4,'ep_1'=4,'tp'=16] {'ep_1'}, dimensions={0}, use_global_device_ids=true | all-gather | bytes 368640 | tf_op jit(solution)/shard_map/all_gather | solution.py:31
  66.9 10.0 %all-gather.1 = bf16[576,256]{1,0:T(8,128)(2,1)S(1)} all-gather(bf16[144,256]{1,0:T(8,128)(2,1)S(1)} %pad_maximum_fusion.6), channel_id=3, replica_groups=mesh['ep_0'=4,'ep_1'=4,'tp'=16] {'ep_0'}, dimensions={0}, use_global_device_ids=true | all-gather | bytes 368640 | tf_op jit(solution)/shard_map/all_gather | solution.py:31
  87.2 1.1 add_bitcast_fusion
  89.5 1.8 multiply_reduce_fusion
  91.3 2.4 fusion.7
  93.7 4.2 %shard_map.167.held_ref = bf16[16,224,2048]{2,1,0:T(8,128)(2,1)} custom-call(bf16[16,64,256]{2,1,0:T(8,128)(2,1)} %bitcast.79, bf16[256,2048]{1,0:T(8,128)(2,1)} %weight_ref.1), custom_call_target="tpu_custom_call" | custom-call | tf_op jit(solution)/shard_map/pallas_call | solution.py:204
  98.0 1.5 pad_maximum_fusion.1.down_ref
  100.1 2.3 pad_maximum_fusion.first_ref
  102.3 3.0 %all-gather.4.cloned.1.call-done.x_ref = bf16[16,160,2176]{2,1,0:T(8,128)(2,1)} async-done(((bf16[1,160,2176]{2,1,0:T(8,128)(2,1)}), bf16[16,160,2176]{2,1,0:T(8,128)(2,1)}) %all-gather.4.cloned.1.call-update) | async-done | bytes 11141136 | tf_op jit(solution)/shard_map/all_gather | solution.py:197
  105.4 16.1 %shard_map.168 = bf16[16,224,2048]{2,1,0:T(8,128)(2,1)} custom-call(bf16[16,160,2176]{2,1,0:T(8,128)(2,1)} %all-gather.4.cloned.1.call-done.x_ref, bf16[2,2048,512]{2,1,0:T(8,128)(2,1)} %pad_maximum_fusion.first_ref, bf16[2,256,2048]{2,1,0:T(8,128)(2,1)S(1)} %pad_maximum_fusion.1.down_ref, ...), custom_call_target="tpu_custom_call", output_to_operand_aliasing={{}: (3, {})} | custom-call | tf_op jit(solution)/shard_map/pallas_call | solution.py:232
  121.5 91.0 %reduce-scatter.2.cloned.1.call-done = bf16[1,224,2048]{2,1,0:T(8,128)(2,1)} async-done(((bf16[16,224,2048]{2,1,0:T(8,128)(2,1)}), bf16[1,224,2048]{2,1,0:T(8,128)(2,1)}) %reduce-scatter.2.cloned.1.call-update) | async-done | bytes 917520 | tf_op jit(solution)/shard_map/reduce_scatter | solution.py:247
  212.5 1.1 slice.251
  214.0 1.2 pad_bitcast_fusion
  215.2 6.5 %all-to-all-start.1 = ((bf16[16,16,2048]{2,1,0:T(8,128)(2,1)}), bf16[16,16,2048]{2,1,0:T(8,128)(2,1)S(1)}, u32[]{:S(2)}, u32[]{:S(2)}) async-start(bf16[16,16,2048]{2,1,0:T(8,128)(2,1)} %pad_bitcast_fusion), calls=%async_computation.2 | async-start | bytes 2097152 | tf_op jit(solution)/shard_map/all_to_all | solution.py:253
  221.7 1.7 slice_bitcast_fusion
  223.4 18.3 %all-to-all-done.1 = bf16[16,16,2048]{2,1,0:T(8,128)(2,1)S(1)} async-done(((bf16[16,16,2048]{2,1,0:T(8,128)(2,1)}), bf16[16,16,2048]{2,1,0:T(8,128)(2,1)S(1)}, u32[]{:S(2)}, u32[]{:S(2)}) %all-to-all-start.1) | async-done | bytes 1048608 | tf_op jit(solution)/shard_map/all_to_all | solution.py:253
  241.7 1.0 convolution_convert_fusion.1
  (75 shorter events, 13.5 us)
Async XLA Ops:
  7.2 42.3 %copy-start = (bf16[1024,256]{1,0:T(8,128)(2,1)S(1)}, bf16[1024,256]{1,0:T(8,128)(2,1)}, u32[]{:S(2)}) copy-start(bf16[1024,256]{1,0:T(8,128)(2,1)} %param.18) | copy-start | bytes 1572868
  7.2 98.2 %all-gather.4.cloned.1.call-start = ((), (), s32[]{:S(2)}) async-start(), calls=%async_computation.3 | async-start | bytes 11837440 | tf_op jit(solution)/shard_map/all_gather | solution.py:197
  11.4 26.4 %copy-start.9 = (f32[1,1024]{1,0:T(1,128)S(1)}, f32[1,1024]{1,0:T(1,128)}, u32[]{:S(2)}) copy-start(f32[1,1024]{1,0:T(1,128)} %param.20) | copy-start | bytes 12292
  11.4 34.7 %copy-start.7 = (bf16[1024,128]{1,0:T(8,128)(2,1)S(1)}, bf16[1024,128]{1,0:T(8,128)(2,1)}, u32[]{:S(2)}) copy-start(bf16[1024,128]{1,0:T(8,128)(2,1)} %param.16) | copy-start | bytes 786436
  12.8 33.3 %copy-start.8 = (bf16[1024,128]{1,0:T(8,128)(2,1)S(1)}, bf16[1024,128]{1,0:T(8,128)(2,1)}, u32[]{:S(2)}) copy-start(bf16[1024,128]{1,0:T(8,128)(2,1)} %param.17) | copy-start | bytes 786436
  37.7 174.8 %reduce-scatter.2.cloned.1.call-start = ((), (), s32[]{:S(2)}) async-start(), calls=%async_computation.4 | async-start | bytes 15597568 | tf_op jit(solution)/shard_map/reduce_scatter | solution.py:247
  77.0 0.7 copy-start.1
  93.7 4.2 %copy-start.4 = (bf16[128,2048]{1,0:T(8,128)(2,1)S(1)}, bf16[128,2048]{1,0:T(8,128)(2,1)}, u32[]{:S(2)}) copy-start(bf16[128,2048]{1,0:T(8,128)(2,1)} %param.31) | copy-start | bytes 1572868
  97.9 1.7 copy-start.5
  97.9 1.8 copy-start.6
  97.9 1.9 copy-start.2
  97.9 2.2 copy-start.3
  215.2 26.5 %all-to-all-start.1 = ((bf16[16,16,2048]{2,1,0:T(8,128)(2,1)}), bf16[16,16,2048]{2,1,0:T(8,128)(2,1)S(1)}, u32[]{:S(2)}, u32[]{:S(2)}) async-start(bf16[16,16,2048]{2,1,0:T(8,128)(2,1)} %pad_bitcast_fusion), calls=%async_computation.2 | async-start | bytes 2097152 | tf_op jit(solution)/shard_map/all_to_all | solution.py:253
Sparse Core Ops, SparseCore 0:
  37.9 67.4 all-gather.3
  121.7 90.7 reduce-scatter.1

commit v2 on v1

v2 whole, which is shorter than its diff:
```python
import jax
import jax.numpy as jnp
from jax import lax
from jax.experimental import pallas as pl
from jax.experimental.pallas import tpu as pltpu
from jax.sharding import Mesh
from jax.sharding import PartitionSpec as P

BLOCK = 128
EP = ("ep_0", "ep_1")
TP = ("z", "core")
EP_TP = EP + TP
LANES = 128
SLOTS = 8
STRIP = 32

epsilon = 1e-06
turn_base = 10000.0
bf16 = jnp.bfloat16
f32 = jnp.float32


def silu(v):
    return v / (1.0 + jnp.exp(-v))


def expert_kernel(x_ref, first_ref, down_ref, held_ref, out_ref):
    del held_ref
    groups, rows, width = x_ref.shape
    model_width = out_ref.shape[-1]
    x = x_ref[...].reshape(groups * rows, width)
    hidden = jnp.dot(x[:, :model_width], first_ref[0], preferred_element_type=f32)
    part = hidden.shape[1] // 4
    extra = x[:, model_width:].astype(f32)
    weight = extra[:, 0:1] + extra[:, 1:2]
    own = extra[:, 2:3]
    routed = silu(hidden[:, :part]) * hidden[:, part : 2 * part] * weight
    shared = silu(hidden[:, 2 * part : 3 * part]) * hidden[:, 3 * part :] * own
    both = jnp.concatenate([routed, shared], axis=1).astype(bf16)
    product = jnp.dot(both, down_ref[0], preferred_element_type=f32)
    out_ref[...] = product.astype(bf16).reshape(out_ref.shape)


def masks():
    row = lax.broadcasted_iota(jnp.int32, (BLOCK, BLOCK), 0)
    column = lax.broadcasted_iota(jnp.int32, (BLOCK, BLOCK), 1)
    return row == column, row >= column


def upright(line, same):
    return jnp.sum(jnp.where(same, line, 0.0), axis=1, keepdims=True)


def advance(state, keys, values, line, column):
    end = line[:, BLOCK - 1 :]
    decayed = (keys.astype(f32) * jnp.exp(end - column)).astype(bf16)
    update = lax.dot_general(
        decayed, values, (((0,), (0,)), ((), ())), preferred_element_type=f32
    )
    return jnp.exp(end) * state + update


def state_kernel(q_ref, k_ref, v_ref, cos_ref, sin_ref, line_ref, qt_ref, kt_ref, out_ref, state_ref, log_ref):
    @pl.when(pl.program_id(0) == 0)
    def _():
        state_ref[...] = jnp.zeros_like(state_ref)
        log_ref[...] = jnp.zeros_like(log_ref)

    cosine, sine = cos_ref[...], sin_ref[...]
    half = q_ref.shape[1] // 2
    q, k = q_ref[...].astype(f32), k_ref[...].astype(f32)
    qt_ref[...] = (q * cosine + pltpu.roll(q, half, 1) * sine).astype(bf16)
    keys = (k * cosine + pltpu.roll(k, half, 1) * sine).astype(bf16)
    kt_ref[...] = keys
    line = line_ref[0]
    same, _ = masks()
    state_ref[...] = advance(state_ref[...], keys, v_ref[...], line, upright(line, same))
    log_ref[...] = log_ref[...] + line[:, BLOCK - 1 :]

    @pl.when(pl.program_id(0) == pl.num_programs(0) - 1)
    def _():
        rows = state_ref.shape[0]
        total = log_ref[...]
        high = total.astype(bf16).astype(f32)
        mark = lax.broadcasted_iota(jnp.int32, total.shape, 0)
        extra = jnp.where(mark == 0, high, jnp.where(mark == 1, total - high, 0.0))
        out_ref[:rows] = state_ref[...].astype(bf16)
        out_ref[rows:] = extra.astype(bf16)


def mixer_kernel(
    place_ref, pieces_ref, q_ref, k_ref, v_ref, gate_ref, line_ref, weight_ref, out_ref, state_ref, mixed_ref
):
    rows = state_ref.shape[0]
    strip = pl.program_id(1)

    @pl.when((pl.program_id(0) == 0) & (strip == 0))
    def _():
        state_ref[...] = jnp.zeros_like(state_ref)

        def enter(k, _):
            log = pieces_ref[k, rows : rows + 16, :].astype(f32)
            decay = jnp.exp(log[0:1, :] + log[1:2, :])
            state_ref[...] = decay * state_ref[...] + pieces_ref[k, :rows, :].astype(f32)
            return 0

        lax.fori_loop(0, place_ref[0], enter, 0)

    @pl.when(strip == 0)
    def _():
        queries, keys, values = q_ref[...], k_ref[...], v_ref[...]
        line = line_ref[0]
        same, lower = masks()
        column = upright(line, same)
        scores = lax.dot_general(
            queries, keys, (((1,), (1,)), ((), ())), preferred_element_type=f32
        )
        spread = jnp.where(lower, column - line, 0.0)
        weights = jnp.where(lower, scores * jnp.exp(spread), 0.0).astype(bf16)
        state = state_ref[...]
        retained = jnp.dot(weights, values, preferred_element_type=f32)
        retained = retained + jnp.dot(
            (queries.astype(f32) * jnp.exp(column)).astype(bf16),
            state.astype(bf16),
            preferred_element_type=f32,
        )
        state_ref[...] = advance(state, keys, values, line, column)
        mean = jnp.mean(retained * retained, axis=1, keepdims=True)
        gated = (silu(gate_ref[...].astype(f32)) * (retained * lax.rsqrt(mean + epsilon))).astype(bf16)
        mixed = jnp.dot(gated, weight_ref[...], preferred_element_type=f32)
        mixed_ref[...] = mixed.astype(bf16)

    for k in range(BLOCK // 2 // STRIP):

        @pl.when(strip == k)
        def _():
            for half in range(2):
                first = half * (BLOCK // 2) + k * STRIP
                out_ref[half] = mixed_ref[first : first + STRIP]


def retention(query_rows, key_rows, value_rows, gate_rows, log_decay, out_weight, rows_before):
    tokens, key_width = query_rows.shape
    value_width = value_rows.shape[1]
    model_width = out_weight.shape[1]
    count = tokens // BLOCK
    ep_count = lax.axis_size(EP)
    members = lax.axis_size(TP)
    start = lax.axis_index(EP) * tokens
    position = (start + jnp.arange(tokens, dtype=jnp.int32)).astype(f32)
    half_width = key_width // 2
    entry = jnp.arange(key_width)
    inverse = turn_base ** (-(entry % half_width).astype(f32) / half_width)
    angles = position[:, None] * inverse[None, :]
    cosine = jnp.cos(angles)
    sine = jnp.where(entry < half_width, -1.0, 1.0) * jnp.sin(angles)
    order = jnp.arange(BLOCK)
    upper = (order[:, None] <= order[None, :]).astype(f32)
    running = jnp.dot(log_decay.reshape(count, BLOCK), upper, precision=lax.Precision.HIGHEST)
    running = running.reshape(count, 1, BLOCK)

    def rows_of(width):
        return pl.BlockSpec((BLOCK, width), lambda n, *_: (n, 0))

    line = pl.BlockSpec((1, 1, BLOCK), lambda n, *_: (n, 0, 0))
    queries, keys, piece = pl.pallas_call(
        state_kernel,
        grid=(count,),
        in_specs=[rows_of(key_width)] * 2 + [rows_of(value_width)] + [rows_of(key_width)] * 2 + [line],
        out_specs=[
            rows_of(key_width),
            rows_of(key_width),
            pl.BlockSpec((key_width + 16, value_width), lambda n: (0, 0)),
        ],
        out_shape=[
            jax.ShapeDtypeStruct((tokens, key_width), bf16),
            jax.ShapeDtypeStruct((tokens, key_width), bf16),
            jax.ShapeDtypeStruct((key_width + 16, value_width), bf16),
        ],
        scratch_shapes=[
            pltpu.VMEM((key_width, value_width), f32),
            pltpu.VMEM((16, value_width), f32),
        ],
    )(query_rows, key_rows, value_rows, cosine, sine, running)
    pieces = lax.all_to_all(
        jnp.broadcast_to(piece, (ep_count,) + piece.shape), EP, split_axis=0, concat_axis=0, tiled=True
    )
    where = jnp.reshape(lax.axis_index(EP), (1,)).astype(jnp.int32)
    strips = BLOCK // 2 // STRIP
    return pl.pallas_call(
        mixer_kernel,
        grid_spec=pltpu.PrefetchScalarGridSpec(
            num_scalar_prefetch=1,
            grid=(count, strips),
            in_specs=[
                pl.BlockSpec(pieces.shape, lambda n, *_: (0, 0, 0)),
                rows_of(key_width),
                rows_of(key_width),
                rows_of(value_width),
                rows_of(value_width),
                line,
                pl.BlockSpec(out_weight.shape, lambda n, *_: (0, 0)),
            ],
            out_specs=pl.BlockSpec(
                (2, STRIP, model_width), lambda n, k, *_: (n, rows_before // STRIP + k, 0)
            ),
            scratch_shapes=[
                pltpu.VMEM((key_width, value_width), f32),
                pltpu.VMEM((BLOCK, model_width), bf16),
            ],
        ),
        out_shape=jax.ShapeDtypeStruct((members, rows_before + tokens // members, model_width), bf16),
        compiler_params=pltpu.CompilerParams(vmem_limit_bytes=40 * 2**20),
    )(where, pieces, queries, keys, value_rows, gate_rows, running, out_weight)


def local(
    query_rows,
    key_rows,
    value_rows,
    gate_rows,
    log_decay,
    out_weight,
    channel_input,
    norm_gain,
    routes,
    route_weight,
    expert_gate,
    expert_up,
    expert_down,
    shared_gate,
    shared_up,
    shared_down,
):
    tokens_dev = query_rows.shape[0]
    tokens_here, topk = routes.shape
    model_width = channel_input.shape[1]
    local_experts, _, hidden_part = expert_gate.shape
    ep_count = lax.axis_size(EP)
    experts_all = ep_count * local_experts
    picks = tokens_here * topk
    capacity = picks // experts_all + max(2, picks // (3 * experts_all))
    slot_count = experts_all * SLOTS

    widened = channel_input.astype(f32)
    normed = (
        widened * lax.rsqrt(jnp.mean(widened * widened, axis=-1, keepdims=True) + epsilon) * norm_gain
    ).astype(bf16)
    flat = routes.reshape(-1)
    order = jnp.arange(picks, dtype=jnp.int32)
    same = (flat[:, None] == flat[None, :]) & (order[None, :] < order[:, None])
    rank = jnp.sum(same.astype(jnp.int32), axis=1)
    slots = ((flat % local_experts) * ep_count + flat // local_experts) * SLOTS + rank
    placing = (jnp.arange(slot_count, dtype=jnp.int32)[:, None] == slots[None, :]).astype(bf16)
    placing_rows = placing.reshape(slot_count, tokens_here, topk).sum(axis=2)
    flat_weight = route_weight.reshape(-1)
    high = flat_weight.astype(bf16)
    low = (flat_weight - high.astype(f32)).astype(bf16)
    mark = (order % topk == 0).astype(bf16)
    lane = jnp.arange(LANES)[None, :]
    extra = jnp.where(
        lane == 0,
        high[:, None],
        jnp.where(lane == 1, low[:, None], jnp.where(lane == 2, mark[:, None], jnp.zeros((), bf16))),
    )
    outgoing = jnp.concatenate(
        [
            jnp.dot(placing_rows, normed, preferred_element_type=f32).astype(bf16),
            jnp.dot(placing, extra, preferred_element_type=f32).astype(bf16),
        ],
        axis=1,
    )
    width = model_width + LANES
    outgoing = outgoing.reshape(local_experts, ep_count, SLOTS, width)
    gathered = []
    for e in range(local_experts):
        arrived = lax.all_to_all(outgoing[e], EP, split_axis=0, concat_axis=0, tiled=True)
        arrived = jnp.transpose(arrived[:, :capacity], (1, 0, 2)).reshape(1, -1, width)
        gathered.append(lax.all_gather(arrived, TP, axis=0, tiled=True))
    each = gathered[0].shape[1]
    routed_rows = local_experts * each

    buffer = retention(
        query_rows, key_rows, value_rows, gate_rows, log_decay, out_weight, routed_rows
    )
    spread = (local_experts,) + shared_gate.shape
    first = jnp.concatenate(
        [
            expert_gate,
            expert_up,
            jnp.broadcast_to(shared_gate, spread),
            jnp.broadcast_to(shared_up, spread),
        ],
        axis=2,
    )
    down = jnp.concatenate(
        [expert_down, jnp.broadcast_to(shared_down, (local_experts,) + shared_down.shape)], axis=1
    )
    groups = 4
    for e in range(local_experts):
        buffer = pl.pallas_call(
            expert_kernel,
            grid=(buffer.shape[0] // groups,),
            in_specs=[
                pl.BlockSpec((groups, each, width), lambda t: (t, 0, 0)),
                pl.BlockSpec((1,) + first.shape[1:], lambda t, e=e: (e, 0, 0)),
                pl.BlockSpec((1,) + down.shape[1:], lambda t, e=e: (e, 0, 0)),
                pl.BlockSpec(memory_space=pl.ANY),
            ],
            out_specs=pl.BlockSpec((groups, each, model_width), lambda t, e=e: (t, e, 0)),
            out_shape=jax.ShapeDtypeStruct(buffer.shape, bf16),
            input_output_aliases={3: 0},
            compiler_params=pltpu.CompilerParams(vmem_limit_bytes=50 * 2**20),
        )(gathered[e], first, down, buffer)

    summed = lax.psum_scatter(buffer, TP, scatter_dimension=0, tiled=True)[0]
    mixer_out = summed[routed_rows:]
    back = summed[:routed_rows].reshape(local_experts, capacity, ep_count, model_width)
    back = jnp.transpose(back, (2, 0, 1, 3))
    back = jnp.pad(back, ((0, 0), (0, 0), (0, SLOTS - capacity), (0, 0)))
    back = back.reshape(ep_count, local_experts * SLOTS, model_width)
    returned = lax.all_to_all(back, EP, split_axis=0, concat_axis=0, tiled=True)
    returned = returned.reshape(slot_count, model_width)
    fetch = placing_rows.reshape(local_experts, ep_count, SLOTS, tokens_here)
    fetch = jnp.transpose(fetch, (1, 0, 2, 3)).reshape(slot_count, tokens_here)
    channel = jnp.dot(fetch.T, returned, preferred_element_type=f32)
    return (mixer_out, channel.astype(bf16))


def solution(mesh):
    cores = 2
    split = Mesh(
        mesh.devices.reshape(4, 4, mesh.shape["tp"] // cores, cores), EP_TP
    )
    return jax.shard_map(
        local,
        mesh=split,
        in_specs=(
            P(EP, TP),
            P(EP, TP),
            P(EP, TP),
            P(EP, TP),
            P(TP, EP),
            P(TP, None),
            P(EP_TP, None),
            P(),
            P(EP_TP, None),
            P(EP_TP, None),
            P(EP, None, TP),
            P(EP, None, TP),
            P(EP, TP, None),
            P(None, TP),
            P(None, TP),
            P(TP, None),
        ),
        out_specs=(P(EP_TP, None), P(EP_TP, None)),
        check_vma=False,
    )
```

time: 250 us -> 255 us (1.020)
  waiting for transfers between devices: 112 us -> 134 us
  between operations: 31.8 us -> 14 us
  Pallas kernels: 20.3 us -> 35.9 us
  blocking collectives: 43.5 us -> 30.9 us
  other arithmetic: 15.9 us -> 9.27 us
  starting transfers between devices: 6.59 us -> 10.3 us
    all_gather x2 -> x0, blocking collectives: 20 us -> none  [carried_in(): pieces = lax.all_gather(packed, axis)]
    pallas_call x2 -> x4, Pallas kernels: 20.3 us -> 35.9 us  [the longest x2 17.9 us: local(): pl.pallas_call(expert_kernel, grid=(buffer.shape[0] // groups,), in_specs...]
    all_gather x1 -> x2, waiting for transfers between devices: 3.03 us -> 17.7 us  [local(): gathered.append(lax.all_gather(arrived, TP, axis=0, tiled=True))]
    all_to_all x0 -> x1, waiting for transfers between devices: none -> 10.5 us  [retention(): lax.all_to_all(jnp.broadcast_to(piece, (ep_count,) + piece.shape), EP, sp...]
    all_to_all x1 -> x2, blocking collectives: 23.5 us -> 30.9 us  [local(): lax.all_to_all(outgoing[e], EP, split_axis=0, concat_axis=0, tiled=True)]
    all_to_all x0 -> x1, starting transfers between devices: none -> 3.7 us  [retention(): lax.all_to_all(jnp.broadcast_to(piece, (ep_count,) + piece.shape), EP, sp...]
    reduce_scatter x1, waiting for transfers between devices: 91 us -> 87.3 us  [local(): summed = lax.psum_scatter(buffer, TP, scatter_dimension=0, tiled=True)[0]]
    another operation x4 -> x0, other arithmetic: 3.34 us -> none
  transfers between devices with their start and end apart: 3 -> 5, of which waited for: 3 -> 4; matrix products, arithmetic and copies ran while one was open for 9% -> 5% of each run, Pallas kernels for 2% -> 11%
where the time goes in v2:
time: 255 us; the launch traced here: 253 us
  waiting for transfers between devices  134 us (53%)
  Pallas kernels  35.9 us (14%)
  blocking collectives  30.9 us (12%)
  local copies, waits for them, and re-layouts  15.8 us (6%)
  between operations  14 us (5%)
  starting transfers between devices  10.3 us (4%)
  other arithmetic  9.27 us (4%)
  matrix products  3.39 us (1%)
    reduce_scatter x1, waiting for transfers between devices, local(): summed = lax.psum_scatter(buffer, TP, scatter_dimension=0, tiled=True)[0]  87.3 us
    all_to_all x2, blocking collectives, local(): lax.all_to_all(outgoing[e], EP, split_axis=0, concat_axis=0, tiled=True)  30.9 us
    all_to_all x1, waiting for transfers between devices, local(): returned = lax.all_to_all(back, EP, split_axis=0, concat_axis=0, tiled=True)  18.2 us
    pallas_call x2, Pallas kernels, local(): pl.pallas_call(expert_kernel, grid=(buffer.shape[0] // groups,), in_specs...  17.9 us
    all_gather x2, waiting for transfers between devices, local(): gathered.append(lax.all_gather(arrived, TP, axis=0, tiled=True))  17.7 us
    pallas_call x1, Pallas kernels, retention(): pl.pallas_call(mixer_kernel, grid_spec=pltpu.PrefetchScalarGridSpec(num_s...  11.2 us
    all_to_all x1, waiting for transfers between devices, retention(): lax.all_to_all(jnp.broadcast_to(piece, (ep_count,) + piece.shape), EP, sp...  10.5 us
    unnamed x31, local copies, waits for them, and re-layouts  7.78 us
  transfers between devices with their start and end apart: 5, of which 4 were waited for; matrix products, arithmetic and copies ran while one was open for 5% of the time, Pallas kernels for 11%

profile of v2, /device:TPU:33, one launch (start us, length us, event | category | flops | bytes accessed | tf_op | source)
XLA Modules:
  0.0 253.4 jit_solution(10384242814115874087)
XLA Ops:
  10.4 1.1 fusion.4
  11.5 1.4 convolution_convert_fusion
  13.3 17.7 %all_to_all.20 = bf16[16,8,2176]{2,1,0:T(8,128)(2,1)S(1)} all-to-all(bf16[16,8,2176]{2,1,0:T(8,128)(2,1)S(1)} %get-tuple-element.8), channel_id=1, replica_groups=mesh['ep_0'=4,'ep_1'=4,'z'=8,'core'=2] {'ep_0','ep_1'}, dimensions={0} | all-to-all | bytes 1114112 | tf_op jit(solution)/shard_map/all_to_all | solution.py:277
  31.9 13.2 %all_to_all.21 = bf16[16,8,2176]{2,1,0:T(8,128)(2,1)S(1)} all-to-all(bf16[16,8,2176]{2,1,0:T(8,128)(2,1)S(1)} %get-tuple-element.9), channel_id=1, replica_groups=mesh['ep_0'=4,'ep_1'=4,'z'=8,'core'=2] {'ep_0','ep_1'}, dimensions={0} | all-to-all | bytes 1114112 | tf_op jit(solution)/shard_map/all_to_all | solution.py:277
  46.6 3.0 %fusion.3 = (f32[1024,128]{1,0:T(8,128)}, f32[1024,128]{1,0:T(8,128)}) fusion(f32[128]{0:T(128)S(1)} %get-tuple-element.16, f32[128]{0:T(128)S(1)} %get-tuple-element.17, f32[1024]{0:T(1024)S(1)} %add_convert_fusion), kind=kLoop, calls=%fused_computation.14 | loop fusion | flops 262144 | bytes 1053696 | tf_op jit(solution)/shard_map/mul | solution.py:156
  49.7 6.7 %shard_map.167 = (bf16[1024,128]{1,0:T(8,128)(2,1)}, bf16[1024,128]{1,0:T(8,128)(2,1)}, bf16[144,256]{1,0:T(8,128)(2,1)}) custom-call(bf16[1024,128]{1,0:T(8,128)(2,1)} %q_ref.1, bf16[1024,128]{1,0:T(8,128)(2,1)} %k_ref.1, bf16[1024,256]{1,0:T(8,128)(2,1)} %v_ref.3, f32[1024,128]{1,0:T(8,128)} %get-tuple-element.11.cos_ref, ...), custom_call_target="tpu_custom_call" | custom-call | tf_op jit(solution)/shard_map/pallas_call | solution.py:166
  56.4 2.0 broadcast_in_dim.93
  58.4 3.7 %all-to-all-start.2 = ((bf16[16,144,256]{2,1,0:T(8,128)(2,1)}), bf16[16,144,256]{2,1,0:T(8,128)(2,1)S(1)}, u32[]{:S(2)}, u32[]{:S(2)}) async-start(bf16[16,144,256]{2,1,0:T(8,128)(2,1)} %broadcast_in_dim.93), calls=%async_computation.2 | async-start | bytes 2359296 | tf_op jit(solution)/shard_map/all_to_all | solution.py:185
  62.4 1.6 pad_maximum_fusion.1.down_ref
  64.0 1.2 broadcast_in_dim.88
  65.3 2.4 pad_maximum_fusion.first_ref
  67.7 10.5 %all-to-all-done.2.pieces_ref = bf16[16,144,256]{2,1,0:T(8,128)(2,1)S(1)} async-done(((bf16[16,144,256]{2,1,0:T(8,128)(2,1)}), bf16[16,144,256]{2,1,0:T(8,128)(2,1)S(1)}, u32[]{:S(2)}, u32[]{:S(2)}) %all-to-all-start.2) | async-done | bytes 1179680 | tf_op jit(solution)/shard_map/all_to_all | solution.py:185
  78.2 1.0 copy-done.1
  79.2 1.2 copy-done.2
  82.4 11.2 %shard_map.168.held_ref = bf16[16,224,2048]{2,1,0:T(8,128)(2,1)} custom-call(s32[1]{0:T(128)} %bitcast.6.place_ref, bf16[16,144,256]{2,1,0:T(8,128)(2,1)S(1)} %all-to-all-done.2.pieces_ref, bf16[1024,128]{1,0:T(8,128)(2,1)S(1)} %copy-done.4, bf16[1024,128]{1,0:T(8,128)(2,1)S(1)} %copy-done.5, bf16[1024,256]{1,0:T(8,128)(2,1)S(1)} %copy-done.1, ...), custom_call_target="tpu_custom_call" | custom-call | tf_op jit(solution)/shard_map/pallas_call | solution.py:190
  93.7 9.0 %shard_map.169.held_ref = bf16[16,224,2048]{2,1,0:T(8,128)(2,1)} custom-call(bf16[16,80,2176]{2,1,0:T(8,128)(2,1)} %all-gather.5.cloned.1.call-done.x_ref, bf16[2,2048,512]{2,1,0:T(8,128)(2,1)} %pad_maximum_fusion.first_ref, bf16[2,256,2048]{2,1,0:T(8,128)(2,1)S(1)} %pad_maximum_fusion.1.down_ref, ...), custom_call_target="tpu_custom_call", output_to_operand_aliasing={{}: (3, {})} | custom-call | tf_op jit(solution)/shard_map/pallas_call | solution.py:301
  102.7 17.7 %all-gather.3.cloned.1.call-done.x_ref = bf16[16,80,2176]{2,1,0:T(8,128)(2,1)} async-done(((bf16[1,80,2176]{2,1,0:T(8,128)(2,1)}), bf16[16,80,2176]{2,1,0:T(8,128)(2,1)}) %all-gather.3.cloned.1.call-update) | async-done | bytes 5570576 | tf_op jit(solution)/shard_map/all_gather | solution.py:279
  120.4 8.9 %shard_map.170 = bf16[16,224,2048]{2,1,0:T(8,128)(2,1)} custom-call(bf16[16,80,2176]{2,1,0:T(8,128)(2,1)} %all-gather.3.cloned.1.call-done.x_ref, bf16[2,2048,512]{2,1,0:T(8,128)(2,1)} %pad_maximum_fusion.first_ref, bf16[2,256,2048]{2,1,0:T(8,128)(2,1)S(1)} %pad_maximum_fusion.1.down_ref, ...), custom_call_target="tpu_custom_call", output_to_operand_aliasing={{}: (3, {})} | custom-call | tf_op jit(solution)/shard_map/pallas_call | solution.py:301
  129.3 87.3 %reduce-scatter.2.cloned.1.call-done = bf16[1,224,2048]{2,1,0:T(8,128)(2,1)} async-done(((bf16[16,224,2048]{2,1,0:T(8,128)(2,1)}), bf16[1,224,2048]{2,1,0:T(8,128)(2,1)}) %reduce-scatter.2.cloned.1.call-update) | async-done | bytes 917520 | tf_op jit(solution)/shard_map/reduce_scatter | solution.py:316
  216.6 1.1 slice.36
  218.1 1.2 pad_bitcast_fusion
  219.3 6.5 %all-to-all-start.3 = ((bf16[16,16,2048]{2,1,0:T(8,128)(2,1)}), bf16[16,16,2048]{2,1,0:T(8,128)(2,1)S(1)}, u32[]{:S(2)}, u32[]{:S(2)}) async-start(bf16[16,16,2048]{2,1,0:T(8,128)(2,1)} %pad_bitcast_fusion), calls=%async_computation.4 | async-start | bytes 2097152 | tf_op jit(solution)/shard_map/all_to_all | solution.py:322
  226.0 1.7 slice_bitcast_fusion
  227.7 18.2 %all-to-all-done.3 = bf16[16,16,2048]{2,1,0:T(8,128)(2,1)S(1)} async-done(((bf16[16,16,2048]{2,1,0:T(8,128)(2,1)}), bf16[16,16,2048]{2,1,0:T(8,128)(2,1)S(1)}, u32[]{:S(2)}, u32[]{:S(2)}) %all-to-all-start.3) | async-done | bytes 1048608 | tf_op jit(solution)/shard_map/all_to_all | solution.py:322
  (61 shorter events, 9.7 us)
Async XLA Ops:
  7.2 38.7 %copy-start = (f32[1,1024]{1,0:T(1,128)S(1)}, f32[1,1024]{1,0:T(1,128)}, u32[]{:S(2)}) copy-start(f32[1,1024]{1,0:T(1,128)} %param.20) | copy-start | bytes 12292
  7.2 86.5 %all-gather.5.cloned.1.call-start = ((), (), s32[]{:S(2)}) async-start(), calls=%async_computation.6 | async-start | bytes 5918720 | tf_op jit(solution)/shard_map/all_gather | solution.py:279
  10.4 2.5 copy-start.11
  31.8 88.6 %all-gather.3.cloned.1.call-start = ((), (), s32[]{:S(2)}) async-start(), calls=%async_computation.5 | async-start | bytes 5918720 | tf_op jit(solution)/shard_map/all_gather | solution.py:279
  45.0 17.2 %copy-start.9 = (bf16[128,2048]{1,0:T(8,128)(2,1)S(1)}, bf16[128,2048]{1,0:T(8,128)(2,1)}, u32[]{:S(2)}) copy-start(bf16[128,2048]{1,0:T(8,128)(2,1)} %param.31) | copy-start | bytes 1572868
  58.4 19.7 %all-to-all-start.2 = ((bf16[16,144,256]{2,1,0:T(8,128)(2,1)}), bf16[16,144,256]{2,1,0:T(8,128)(2,1)S(1)}, u32[]{:S(2)}, u32[]{:S(2)}) async-start(bf16[16,144,256]{2,1,0:T(8,128)(2,1)} %broadcast_in_dim.93), calls=%async_computation.2 | async-start | bytes 2359296 | tf_op jit(solution)/shard_map/all_to_all | solution.py:185
  62.2 154.5 %reduce-scatter.2.cloned.1.call-start = ((), (), s32[]{:S(2)}) async-start(), calls=%async_computation.7 | async-start | bytes 15597568 | tf_op jit(solution)/shard_map/reduce_scatter | solution.py:316
  62.2 3.0 %copy-start.10 = (bf16[2048,128]{1,0:T(8,128)(2,1)S(1)}, bf16[2048,128]{1,0:T(8,128)(2,1)}, u32[]{:S(2)}) copy-start(bf16[2048,128]{1,0:T(8,128)(2,1)} %param.30) | copy-start | bytes 1572868
  62.2 3.1 %copy-start.7 = (bf16[2,2048,128]{2,1,0:T(8,128)(2,1)S(1)}, bf16[2,2048,128]{2,1,0:T(8,128)(2,1)}, u32[]{:S(2)}) copy-start(bf16[2,2048,128]{2,1,0:T(8,128)(2,1)} %param.27) | copy-start | bytes 3145732
  62.2 3.1 %copy-start.8 = (bf16[2,2048,128]{2,1,0:T(8,128)(2,1)S(1)}, bf16[2,2048,128]{2,1,0:T(8,128)(2,1)}, u32[]{:S(2)}) copy-start(bf16[2,2048,128]{2,1,0:T(8,128)(2,1)} %param.26) | copy-start | bytes 3145732
  65.3 12.9 %copy-start.4 = (bf16[1024,128]{1,0:T(8,128)(2,1)S(1)}, bf16[1024,128]{1,0:T(8,128)(2,1)}, u32[]{:S(2)}) copy-start(bf16[1024,128]{1,0:T(8,128)(2,1)} %get-tuple-element.6.q_ref) | copy-start | bytes 786436
  65.3 12.8 %copy-start.6 = (f32[128,8]{0,1:T(8,128)S(1)}, f32[128,8]{0,1:T(8,128)}, u32[]{:S(2)}) copy-start(f32[128,8]{0,1:T(8,128)} %fusion.12) | copy-start | bytes 12292
  78.2 1.0 copy-start.1
  79.2 1.2 copy-start.2
  80.4 1.0 copy-start.3
  81.5 0.9 copy-start.5
  129.3 96.6 %copy-start.12 = (bf16[256,48]{0,1:T(8,128)(2,1)S(1)}, bf16[256,48]{0,1:T(8,128)(2,1)}, u32[]{:S(2)}) copy-start(bf16[256,48]{0,1:T(8,128)(2,1)} %copy-done.11) | copy-start | bytes 73732
  219.3 26.5 %all-to-all-start.3 = ((bf16[16,16,2048]{2,1,0:T(8,128)(2,1)}), bf16[16,16,2048]{2,1,0:T(8,128)(2,1)S(1)}, u32[]{:S(2)}, u32[]{:S(2)}) async-start(bf16[16,16,2048]{2,1,0:T(8,128)(2,1)} %pad_bitcast_fusion), calls=%async_computation.4 | async-start | bytes 2097152 | tf_op jit(solution)/shard_map/all_to_all | solution.py:322
Sparse Core Ops, SparseCore 0:
  31.9 44.0 all-gather.4
  77.8 42.4 all-gather.2
  129.4 87.1 reduce-scatter.1
